TPU v7x, 512 devices: a whole 4x4x16 slice. The times are simulated.
512 devices in a mesh: ep: 32 (over z, core), tp: 16 (over y, x).
Axes of the slice: x: 4, y: 4, z: 16, core: 2. Of those that a mesh axis runs over, the one named last changes fastest.
Arguments:
- mix_in: bfloat16 [8192, 2048], P('ep'), may hold values from -6 to 6
- mix_gain: float32 [2048], replicated, may hold values from 0.1 to 1.9
- w_in_x: bfloat16 [2048, 2048], P(None, 'tp'), may hold values from -0.125 to 0.125
- w_in_y: bfloat16 [2048, 2048], P(None, 'tp'), may hold values from -0.125 to 0.125
- conv_taps: float32 [4, 2048], P(None, 'tp'), may hold values from -3 to 3
- recur_gate_w: bfloat16 [16, 128, 128], P('tp'), may hold values from -0.5 to 0.5
- input_gate_w: bfloat16 [16, 128, 128], P('tp'), may hold values from -0.5 to 0.5
- decay_logit: float32 [2048], P('tp'), may hold values from 4 to 20
- decay_shift: float32 [8192, 2048], P('ep', 'tp'), may hold values from -2.2 to 0
- moe_in: bfloat16 [8192, 2048], P('ep'), may hold values from -6 to 6
- moe_gain: float32 [2048], replicated, may hold values from 0.1 to 1.9
- routes: int32 [8192, 2], P('ep'), may hold values from 0 to 31, all different within a row; in each aligned block of 256 rows (0 to 255, 256 to 511, ...) at most 32 rows name the same one
- route_weight: float32 [8192, 2], P('ep'), may hold values from 0.1 to 1
- expert_gate: bfloat16 [32, 2048, 2048], P('ep', None, 'tp'), may hold values from -0.125 to 0.125
- expert_up: bfloat16 [32, 2048, 2048], P('ep', None, 'tp'), may hold values from -0.125 to 0.125
- expert_down: bfloat16 [32, 2048, 2048], P('ep', None, 'tp'), may hold values from -0.125 to 0.125
Outputs:
- mixer_out: bfloat16 [8192, 2048], P('ep', 'tp')
- moe_out: bfloat16 [8192, 2048], P('ep', 'tp')
Inputs may be any that keep to these rules, and one draw needn't show every extreme that they name: `routes`: each row names 2 different experts. Among the rows of one index of ep no expert is named more than 32 times, a bound that some block reaches.
All inputs are finite; a program needn't handle non-finite values.
Results may differ from a plain program's by a relative error of at most 0.0095.
Values may be sent and summed in bfloat16 or wider, within the bound.
A program may use at most 64 MiB of HBM per device.

v0:
```python
import jax
import jax.numpy as jnp
from jax import lax
from jax.sharding import PartitionSpec as P

epsilon = 1e-06
lru_scale = 8.0


def from_behind(value, axis, by):
    count = lax.axis_size(axis)
    pairs = [(i, i + by) for i in range(count) if 0 <= i + by < count]
    return lax.ppermute(value, axis, pairs)


def copy_for_each(value, axis):
    count = lax.axis_size(axis)
    return lax.all_to_all(
        jnp.broadcast_to(value[None], (count, *value.shape)), axis, 0, 0, tiled=True
    )


def all_in_one(value, axis):
    leaves = jax.tree.leaves(value)
    sequence = sorted(range(len(leaves)), key=lambda k: -leaves[k].size)
    width = (1, *leaves[sequence[0]].shape)[-1]
    lines = [
        jnp.pad(leaves[k].reshape(-1), (0, -leaves[k].size % width)).reshape(-1, width)
        for k in sequence
    ]
    both, at, found = (copy_for_each(jnp.concatenate(lines), axis), 0, {})
    for k, line in zip(sequence, lines):
        slab = both[:, at : at + len(line)].reshape(len(both), -1)
        found[k] = slab[:, : leaves[k].size].reshape(-1, *leaves[k].shape)
        at += len(line)
    numbers = iter(range(len(leaves)))
    return jax.tree.map(lambda _: found[next(numbers)], value)


def combined_pairwise(pieces, combine):
    while len(jax.tree.leaves(pieces)[0]) > 1:
        pieces = jax.vmap(combine)(
            *(jax.tree.map(lambda part: part[side::2], pieces) for side in (0, 1))
        )
    return jax.tree.map(lambda part: part[0], pieces)


def entering(value, axis, combine, identity):
    count, index = (lax.axis_size(axis), lax.axis_index(axis))
    passed = jnp.arange(count) < index

    def kept(part, zero, own):
        part = jnp.where(
            passed.reshape(-1, *(1 for _ in own.shape)), part, jnp.asarray(zero, own.dtype)
        )
        return part

    pieces = all_in_one(value, axis)
    return combined_pairwise(jax.tree.map(kept, pieces, identity, value), combine)


def norm_rows(rows, gain):
    widened = rows.astype(jnp.float32)
    scaled = widened * lax.rsqrt(jnp.mean(widened * widened, axis=-1, keepdims=True) + epsilon)
    return (scaled * gain[None, :]).astype(jnp.bfloat16)


def link(earlier, later):
    return (earlier[0] * later[0], later[0] * earlier[1] + later[1])


def local(
    mix_in,
    mix_gain,
    w_in_x,
    w_in_y,
    conv_taps,
    recur_gate_w,
    input_gate_w,
    decay_logit,
    decay_shift,
    moe_in,
    moe_gain,
    routes,
    route_weight,
    expert_gate,
    expert_up,
    expert_down,
):
    row_count = mix_in.shape[0]
    width_dev = w_in_x.shape[1]
    heads_dev = recur_gate_w.shape[0]
    block_size = recur_gate_w.shape[1]
    tap_count = conv_taps.shape[0]
    mixer_rows = norm_rows(mix_in, mix_gain)
    x_branch = jnp.dot(mixer_rows, w_in_x, preferred_element_type=jnp.float32).astype(jnp.bfloat16)
    y_branch = jnp.dot(mixer_rows, w_in_y, preferred_element_type=jnp.float32).astype(jnp.bfloat16)
    previous = from_behind(x_branch[row_count - (tap_count - 1) :], "ep", 1)
    padded = jnp.concatenate([previous, x_branch], axis=0)
    conv_sum = jnp.zeros((row_count, width_dev), jnp.float32)
    for tap_index in range(tap_count):
        conv_sum = conv_sum + conv_taps[tap_index][None, :] * padded[
            tap_index : tap_index + row_count
        ].astype(jnp.float32)
    x_conv = conv_sum.astype(jnp.bfloat16)
    heads_in = x_conv.reshape(row_count, heads_dev, block_size)
    gate_a = jnp.einsum(
        "thi,hij->thj", heads_in, recur_gate_w, preferred_element_type=jnp.float32
    ).reshape(row_count, width_dev)
    gate_x = jnp.einsum(
        "thi,hij->thj", heads_in, input_gate_w, preferred_element_type=jnp.float32
    ).reshape(row_count, width_dev)
    log_decay = (
        -lru_scale * jax.nn.sigmoid(gate_a) * jax.nn.softplus(-decay_logit)[None, :] + decay_shift
    )
    lru_drive = (
        jnp.sqrt(-jnp.expm1(2.0 * log_decay)) * jax.nn.sigmoid(gate_x) * x_conv.astype(jnp.float32)
    )
    through, local_state = lax.associative_scan(link, (jnp.exp(log_decay), lru_drive), axis=0)
    identity = (jnp.ones((width_dev,), jnp.float32), jnp.zeros((width_dev,), jnp.float32))
    carried = entering((through[row_count - 1], local_state[row_count - 1]), "ep", link, identity)
    lru_state = local_state + through * carried[1][None, :]
    mixer_out = (lru_state * jax.nn.gelu(y_branch.astype(jnp.float32))).astype(jnp.bfloat16)
    moe_rows = norm_rows(moe_in, moe_gain)
    token_count = moe_rows.shape[0]
    feature_count = moe_rows.shape[1]
    choose_count = routes.shape[1]
    expert_count = lax.axis_size("ep")
    capacity = 2 * token_count * choose_count // expert_count
    slot_total = expert_count * capacity
    expert_ids = routes.reshape(-1)
    onehot = (expert_ids[:, None] == jnp.arange(expert_count, dtype=jnp.int32)[None, :]).astype(
        jnp.int32
    )
    slot_rank = jnp.sum(jnp.cumsum(onehot, axis=0) * onehot, axis=1) - 1
    slot_index = expert_ids * capacity + slot_rank
    token_index = jnp.repeat(jnp.arange(token_count, dtype=jnp.int32), choose_count)
    slot_owner = jnp.full((slot_total,), token_count, jnp.int32).at[slot_index].set(token_index)
    padded_rows = jnp.concatenate([moe_rows, jnp.zeros((1, feature_count), jnp.bfloat16)], axis=0)
    outgoing = padded_rows[slot_owner].reshape(expert_count, capacity, feature_count)
    column_width = feature_count // lax.axis_size("tp")
    own_columns = lax.dynamic_slice_in_dim(
        outgoing, lax.axis_index("tp") * column_width, column_width, 2
    )
    incoming = lax.all_to_all(own_columns, "ep", split_axis=0, concat_axis=0, tiled=True)
    piece = lax.all_gather(incoming, "tp", axis=2, tiled=True)
    flat_rows = piece.reshape(slot_total, piece.shape[2])
    gate_rows = expert_gate[0]
    up_rows = expert_up[0]
    gate_proj = jnp.dot(flat_rows, gate_rows, preferred_element_type=jnp.float32)
    up_proj = jnp.dot(flat_rows, up_rows, preferred_element_type=jnp.float32)
    hidden = (jax.nn.silu(gate_proj) * up_proj).astype(jnp.bfloat16)
    down_rows = expert_down[0]
    columns = jnp.dot(
        lax.all_gather(hidden, "tp", axis=1, tiled=True),
        down_rows,
        preferred_element_type=jnp.float32,
    )
    results = columns.astype(jnp.bfloat16).reshape(expert_count, capacity, expert_down.shape[2])
    returned = lax.all_to_all(results, "ep", split_axis=0, concat_axis=0, tiled=True).reshape(
        slot_total, expert_down.shape[2]
    )
    picked = (
        returned[slot_index]
        .astype(jnp.float32)
        .reshape(token_count, choose_count, expert_down.shape[2])
    )
    route_share = route_weight / jnp.sum(route_weight, axis=1, keepdims=True)
    moe_out = jnp.sum(route_share[:, :, None] * picked, axis=1).astype(jnp.bfloat16)
    return (mixer_out, moe_out)


def solution(mesh):
    placed = (
        P("ep", None),
        P(),
        P(None, "tp"),
        P(None, "tp"),
        P(None, "tp"),
        P("tp", None, None),
        P("tp", None, None),
        P("tp"),
        P("ep", "tp"),
        P("ep", None),
        P(),
        P("ep", None),
        P("ep", None),
        P("ep", None, "tp"),
        P("ep", None, "tp"),
        P("ep", None, "tp"),
    )
    return jax.shard_map(
        local, mesh=mesh, in_specs=placed, out_specs=(P("ep", "tp"), P("ep", "tp")), check_vma=False
    )
```

profile of v0, /device:TPU:1, one launch (start us, length us, event | category | flops | bytes accessed | tf_op | source)
XLA Modules:
  0.0 251.2 jit_solution(5826928221437767677)
XLA Ops:
  7.2 0.0 copy-start
  7.2 0.0 copy-start.2
  7.2 0.0 all-gather.3.cloned.1.call-start
  7.3 0.9 copy.27
  8.2 0.1 eq.29
  8.3 0.1 eq.25
  8.5 0.7 broadcast_multiply_fusion
  9.2 1.2 reduce-window.6
  10.3 0.2 slice_reduce_fusion
  10.6 0.1 fusion.43
  10.7 0.1 copy.26
  10.9 0.1 mul.375
  11.0 0.1 reshape.156
  11.2 2.4 scatter_custom_fusion
  13.6 1.5 fusion.3
  15.2 0.3 fusion.5
  15.5 0.1 concatenate.67
  15.6 0.0 copy-start.3
  15.6 6.0 %gather_fusion = bf16[1024,2048]{1,0:T(8,128)(2,1)} fusion(bf16[257,2048]{1,0:T(8,128)(2,1)S(1)} %concatenate.67, s32[1024]{0:T(1024)S(1)} %fusion.51), kind=kCustom, calls=%fused_computation | custom fusion | bytes 8392704 | tf_op jit(solution)/shard_map/gather | solution.py:140
  21.6 1.0 constant_dynamic-slice_fusion
  22.6 0.0 copy-start.5
  22.6 38.9 %all_to_all.15 = bf16[32,32,128]{2,1,0:T(8,128)(2,1)} all-to-all(bf16[32,32,128]{2,1,0:T(8,128)(2,1)S(1)} %constant_dynamic-slice_fusion), channel_id=1, replica_groups=mesh['ep'=32,'tp'=16] {'ep'}, dimensions={0} | all-to-all | bytes 524288 | tf_op jit(solution)/shard_map/all_to_all | solution.py:145
  61.5 0.0 all-gather.3.cloned.1.call-update
  61.5 0.0 all-gather.5.cloned.1.call-start
  61.6 0.3 fusion
  61.9 0.5 convolution_convert_fusion.2
  62.4 2.2 collective-permute-start
  64.7 59.1 %all-gather.3.cloned.1.call-done = bf16[32,32,2048]{2,1,0:T(8,128)(2,1)} async-done(((bf16[32,32,128]{2,1,0:T(8,128)(2,1)}), bf16[32,32,2048]{2,1,0:T(8,128)(2,1)}) %all-gather.3.cloned.1.call-update) | async-done | bytes 4194320 | tf_op jit(solution)/shard_map/all_gather | solution.py:146
  123.8 3.6 %fusion.20 = f32[1024,128]{1,0:T(8,128)S(1)} fusion(bf16[1024,2048]{1,0:T(8,128)(2,1)} %bitcast.61, bf16[1,2048,128]{2,1,0:T(8,128)(2,1)S(1)} %copy-done), kind=kOutput, calls=%fused_computation.33 | convolution fusion | flops 536870912 | bytes 5242880 | tf_op jit(solution)/shard_map/dot_general | solution.py:150
  127.4 0.0 copy-start.15
  127.4 0.0 copy-start.11
  127.4 2.0 fusion.6
  129.4 0.0 all-gather.5.cloned.1.call-update
  129.5 0.1 add_convert_fusion
  129.6 0.2 fusion.61
  129.8 0.2 fusion.16
  132.0 0.6 broadcast_in_dim.27
  132.6 14.4 %all-to-all-start = ((f32[32,2,128]{2,1,0:T(2,128)}), f32[32,2,128]{2,1,0:T(2,128)S(1)}, u32[]{:S(2)}, u32[]{:S(2)}) async-start(f32[32,2,128]{2,1,0:T(2,128)} %broadcast_in_dim.27), calls=%async_computation | async-start | bytes 65536 | tf_op jit(solution)/shard_map/all_to_all | solution.py:18
  147.0 0.1 copy.25
  147.2 11.9 %all-to-all-done = f32[32,2,128]{2,1,0:T(2,128)S(1)} async-done(((f32[32,2,128]{2,1,0:T(2,128)}), f32[32,2,128]{2,1,0:T(2,128)S(1)}, u32[]{:S(2)}, u32[]{:S(2)}) %all-to-all-start) | async-done | bytes 32800 | tf_op jit(solution)/shard_map/all_to_all | solution.py:18
  159.1 0.1 broadcast_select_fusion.1
  159.3 41.9 %all-gather.5.cloned.1.call-done = bf16[1024,2048]{1,0:T(8,128)(2,1)} async-done(((bf16[1024,128]{1,0:T(8,128)(2,1)}), bf16[1024,2048]{1,0:T(8,128)(2,1)}) %all-gather.5.cloned.1.call-update) | async-done | bytes 4194320 | tf_op jit(solution)/shard_map/all_gather | solution.py:155
  201.2 4.1 %convolution_convert_fusion = bf16[1024,128]{1,0:T(8,128)(2,1)} fusion(bf16[1024,2048]{1,0:T(8,128)(2,1)} %all-gather.5.cloned.1.call-done, bf16[1,2048,128]{2,1,0:T(8,128)(2,1)S(1)} %copy-done.9), kind=kOutput, calls=%fused_computation.15 | convolution fusion | flops 537001984 | bytes 4980736 | tf_op jit(solution)/shard_map/dot_general | solution.py:154
  205.3 14.4 %all-to-all-start.2 = ((bf16[32,32,128]{2,1,0:T(8,128)(2,1)}), bf16[32,32,128]{2,1,0:T(8,128)(2,1)S(1)}, u32[]{:S(2)}, u32[]{:S(2)}) async-start(bf16[32,32,128]{2,1,0:T(8,128)(2,1)} %bitcast.17), calls=%async_computation.2 | async-start | bytes 524288 | tf_op jit(solution)/shard_map/all_to_all | solution.py:160
  220.0 1.1 fusion.37
  221.1 20.9 %all-to-all-done.2 = bf16[32,32,128]{2,1,0:T(8,128)(2,1)S(1)} async-done(((bf16[32,32,128]{2,1,0:T(8,128)(2,1)}), bf16[32,32,128]{2,1,0:T(8,128)(2,1)S(1)}, u32[]{:S(2)}, u32[]{:S(2)}) %all-to-all-start.2) | async-done | bytes 262176 | tf_op jit(solution)/shard_map/all_to_all | solution.py:160
  242.0 1.3 gather_fusion.1
  243.3 1.1 fusion.24
  (190 shorter events, 1.8 us)
Async XLA Ops:
  7.2 116.6 %copy-start = (bf16[1,2048,128]{2,1,0:T(8,128)(2,1)S(1)}, bf16[1,2048,128]{2,1,0:T(8,128)(2,1)}, u32[]{:S(2)}) copy-start(bf16[1,2048,128]{2,1,0:T(8,128)(2,1)} %param.29) | copy-start | bytes 1572868
  7.2 8.0 %copy-start.2 = (bf16[256,2048]{1,0:T(8,128)(2,1)S(1)}, bf16[256,2048]{1,0:T(8,128)(2,1)}, u32[]{:S(2)}) copy-start(bf16[256,2048]{1,0:T(8,128)(2,1)} %param.25) | copy-start | bytes 3145732
  7.2 8.0 %copy-start.4 = (f32[2048]{0:T(1024)S(1)}, f32[2048]{0:T(1024)}, u32[]{:S(2)}) copy-start(f32[2048]{0:T(1024)} %param.26) | copy-start | bytes 24580
  7.2 116.6 %all-gather.3.cloned.1.call-start = ((), (), s32[]{:S(2)}) async-start(), calls=%async_computation.3 | async-start | bytes 4456448 | tf_op jit(solution)/shard_map/all_gather | solution.py:146
  15.6 46.0 %copy-start.3 = (bf16[256,2048]{1,0:T(8,128)(2,1)S(1)}, bf16[256,2048]{1,0:T(8,128)(2,1)}, u32[]{:S(2)}) copy-start(bf16[256,2048]{1,0:T(8,128)(2,1)} %param.16) | copy-start | bytes 3145732
  21.6 40.3 %copy-start.7 = (bf16[2048,128]{1,0:T(8,128)(2,1)S(1)}, bf16[2048,128]{1,0:T(8,128)(2,1)}, u32[]{:S(2)}) copy-start(bf16[2048,128]{1,0:T(8,128)(2,1)} %param.18) | copy-start | bytes 1572868
  21.6 40.3 %copy-start.14 = (f32[2048]{0:T(1024)S(1)}, f32[2048]{0:T(1024)}, u32[]{:S(2)}) copy-start(f32[2048]{0:T(1024)} %param.17) | copy-start | bytes 24580
  22.6 42.1 %copy-start.5 = (f32[256,2]{0,1:T(2,128)S(1)}, f32[256,2]{0,1:T(2,128)}, u32[]{:S(2)}) copy-start(f32[256,2]{0,1:T(2,128)} %param.28) | copy-start | bytes 6148
  61.5 139.6 %all-gather.5.cloned.1.call-start = ((), (), s32[]{:S(2)}) async-start(), calls=%async_computation.4 | async-start | bytes 4456448 | tf_op jit(solution)/shard_map/all_gather | solution.py:155
  62.4 67.1 %collective-permute-start = (bf16[3,128]{1,0:T(4,128)(2,1)S(1)}, bf16[3,128]{1,0:T(4,128)(2,1)S(1)}, u32[]{:S(2)}, u32[]{:S(2)}) collective-permute-start(bf16[3,128]{1,0:T(4,128)(2,1)S(1)} %slice.443), channel_id=1, source_target_pairs={{0,16},{16,32},{32,48},{48,64},{64,80},{80,96},{96,112},{112,128},... | collective-permute-start | bytes 2312 | tf_op jit(solution)/shard_map/ppermute | solution.py:13
  123.8 3.6 %copy-start.1 = (bf16[32,32,2048]{2,1,0:T(8,128)(2,1)S(1)}, bf16[32,32,2048]{2,1,0:T(8,128)(2,1)}, u32[]{:S(2)}) copy-start(bf16[32,32,2048]{2,1,0:T(8,128)(2,1)} %all-gather.3.cloned.1.call-done) | copy-start | bytes 12582916
  123.8 3.6 %copy-start.8 = (bf16[1,2048,128]{2,1,0:T(8,128)(2,1)S(1)}, bf16[1,2048,128]{2,1,0:T(8,128)(2,1)}, u32[]{:S(2)}) copy-start(bf16[1,2048,128]{2,1,0:T(8,128)(2,1)} %param.30) | copy-start | bytes 1572868
  127.4 2.1 copy-start.6
  127.4 2.1 copy-start.15
  127.4 2.2 copy-start.11
  127.4 2.2 copy-start.12
  127.4 2.4 copy-start.13
  131.3 69.8 %copy-start.9 = (bf16[1,2048,128]{2,1,0:T(8,128)(2,1)S(1)}, bf16[1,2048,128]{2,1,0:T(8,128)(2,1)}, u32[]{:S(2)}) copy-start(bf16[1,2048,128]{2,1,0:T(8,128)(2,1)} %param.31) | copy-start | bytes 1572868
  132.6 26.4 %all-to-all-start = ((f32[32,2,128]{2,1,0:T(2,128)}), f32[32,2,128]{2,1,0:T(2,128)S(1)}, u32[]{:S(2)}, u32[]{:S(2)}) async-start(f32[32,2,128]{2,1,0:T(2,128)} %broadcast_in_dim.27), calls=%async_computation | async-start | bytes 65536 | tf_op jit(solution)/shard_map/all_to_all | solution.py:18
  159.3 60.7 %copy-start.10 = (bf16[2048,128]{1,0:T(8,128)(2,1)S(1)}, bf16[2048,128]{1,0:T(8,128)(2,1)}, u32[]{:S(2)}) copy-start(bf16[2048,128]{1,0:T(8,128)(2,1)} %param.19) | copy-start | bytes 1572868
  205.3 36.6 %all-to-all-start.2 = ((bf16[32,32,128]{2,1,0:T(8,128)(2,1)}), bf16[32,32,128]{2,1,0:T(8,128)(2,1)S(1)}, u32[]{:S(2)}, u32[]{:S(2)}) async-start(bf16[32,32,128]{2,1,0:T(8,128)(2,1)} %bitcast.17), calls=%async_computation.2 | async-start | bytes 524288 | tf_op jit(solution)/shard_map/all_to_all | solution.py:160
Sparse Core Ops, SparseCore 0:
  61.7 62.0 all-gather.2
  129.6 71.5 all-gather.4
where the time goes:
time: 252 us; the launch traced here: 251 us
  waiting for transfers between devices  134 us (53%)
  blocking collectives  38.9 us (15%)
  starting transfers between devices  31.1 us (12%)
  between operations  15.2 us (6%)
  local copies, waits for them, and re-layouts  14.7 us (6%)
  matrix products  11.7 us (5%)
  other arithmetic  5.83 us (2%)
    all_gather x1, waiting for transfers between devices, local(): piece = lax.all_gather(incoming, 'tp', axis=2, tiled=True)  59.1 us
    all_gather x1, waiting for transfers between devices, local(): lax.all_gather(hidden, 'tp', axis=1, tiled=True)  41.9 us
    all_to_all x1, blocking collectives, local(): lax.all_to_all(own_columns, 'ep', split_axis=0, concat_axis=0, tiled=True)  38.9 us
    all_to_all x1, waiting for transfers between devices, local(): lax.all_to_all(results, 'ep', split_axis=0, concat_axis=0, tiled=True)  20.9 us
    all_to_all x1, starting transfers between devices, copy_for_each(): lax.all_to_all(jnp.broadcast_to(value[None], (count, *value.shape)), axis...  14.4 us
    all_to_all x1, starting transfers between devices, local(): lax.all_to_all(results, 'ep', split_axis=0, concat_axis=0, tiled=True)  14.4 us
    all_to_all x1, waiting for transfers between devices, copy_for_each(): lax.all_to_all(jnp.broadcast_to(value[None], (count, *value.shape)), axis...  11.9 us
    gather x1, local copies, waits for them, and re-layouts, local(): padded_rows[slot_owner].reshape(expert_count, capacity, feature_count)  5.97 us
  transfers between devices with their start and end apart: 5, of which 4 were waited for; matrix products, arithmetic and copies ran while one was open for 4% of the time, Pallas kernels for 0%

commit v1 on v0

--- a/solution.py
+++ b/solution.py
@@ -5,6 +5,22 @@
 
 epsilon = 1e-06
 lru_scale = 8.0
+
+
+def collect(x, axis, dim):
+    ways, here, step = (lax.axis_size(axis), lax.axis_index(axis), x.shape[dim])
+    shape = [n * ways if d == dim else n for d, n in enumerate(x.shape)]
+    full = lax.dynamic_update_slice_in_dim(jnp.zeros(shape, x.dtype), x, here * step, axis=dim)
+    going_up = going_down = x
+    for far in range(1, ways // 2 + 1):
+        going_up = lax.ppermute(going_up, axis, [(d, (d + 1) % ways) for d in range(ways)])
+        full = lax.dynamic_update_slice_in_dim(full, going_up, (here - far) % ways * step, axis=dim)
+        if 2 * far < ways:
+            going_down = lax.ppermute(going_down, axis, [(d, (d - 1) % ways) for d in range(ways)])
+            full = lax.dynamic_update_slice_in_dim(
+                full, going_down, (here + far) % ways * step, axis=dim
+            )
+    return full
 
 
 def from_behind(value, axis, by):
@@ -151,11 +167,7 @@
     up_proj = jnp.dot(flat_rows, up_rows, preferred_element_type=jnp.float32)
     hidden = (jax.nn.silu(gate_proj) * up_proj).astype(jnp.bfloat16)
     down_rows = expert_down[0]
-    columns = jnp.dot(
-        lax.all_gather(hidden, "tp", axis=1, tiled=True),
-        down_rows,
-        preferred_element_type=jnp.float32,
-    )
+    columns = jnp.dot(collect(hidden, "tp", 1), down_rows, preferred_element_type=jnp.float32)
     results = columns.astype(jnp.bfloat16).reshape(expert_count, capacity, expert_down.shape[2])
     returned = lax.all_to_all(results, "ep", split_axis=0, concat_axis=0, tiled=True).reshape(
         slot_total, expert_down.shape[2]

time: 252 us -> 293 us (1.16)
  starting transfers between devices: 31.1 us -> 98.9 us
  waiting for transfers between devices: 134 us -> 88.2 us
  local copies, waits for them, and re-layouts: 14.7 us -> 30.2 us
    ppermute x0 -> x15, starting transfers between devices: none -> 64.3 us  [the longest x7 47.9 us: collect(): lax.ppermute(going_down, axis, [(d, (d - 1) % ways) for d in range(ways)])]
    all_gather x1 -> x0, waiting for transfers between devices: 41.9 us -> none  [local(): lax.all_gather(hidden, 'tp', axis=1, tiled=True)]
    dynamic_update_slice x0 -> x15, local copies, waits for them, and re-layouts: none -> 12.3 us  [the longest x8 7.02 us: collect(): lax.dynamic_update_slice_in_dim(full, going_up, (here - far) % ways * ste...]
    ppermute x0 -> x15, waiting for transfers between devices: none -> 10.2 us  [the longest x8 7.76 us: collect(): lax.ppermute(going_up, axis, [(d, (d + 1) % ways) for d in range(ways)])]
    all_to_all x1, waiting for transfers between devices: 11.9 us -> 2.64 us  [copy_for_each(): lax.all_to_all(jnp.broadcast_to(value[None], (count, *value.shape)), axis...]
    all_gather x1, waiting for transfers between devices: 59.1 us -> 54.8 us  [local(): piece = lax.all_gather(incoming, 'tp', axis=2, tiled=True)]
  transfers between devices with their start and end apart: 5 -> 19, of which waited for: 4 -> 8; matrix products, arithmetic and copies ran while one was open for 4% -> 6% of each run, Pallas kernels for 0% -> 0%
where the time goes in v1:
time: 293 us; the launch traced here: 292 us
  starting transfers between devices  98.9 us (34%)
  waiting for transfers between devices  88.2 us (30%)
  blocking collectives  38.9 us (13%)
  local copies, waits for them, and re-layouts  30.2 us (10%)
  between operations  15.7 us (5%)
  matrix products  13.2 us (5%)
  other arithmetic  7.05 us (2%)
    all_gather x1, waiting for transfers between devices, local(): piece = lax.all_gather(incoming, 'tp', axis=2, tiled=True)  54.8 us
    ppermute x7, starting transfers between devices, collect(): lax.ppermute(going_down, axis, [(d, (d - 1) % ways) for d in range(ways)])  47.9 us
    all_to_all x1, blocking collectives, local(): lax.all_to_all(own_columns, 'ep', split_axis=0, concat_axis=0, tiled=True)  38.9 us
    all_to_all x1, waiting for transfers between devices, local(): lax.all_to_all(results, 'ep', split_axis=0, concat_axis=0, tiled=True)  19.8 us
    all_to_all x1, starting transfers between devices, local(): lax.all_to_all(results, 'ep', split_axis=0, concat_axis=0, tiled=True)  16.9 us
    ppermute x8, starting transfers between devices, collect(): lax.ppermute(going_up, axis, [(d, (d + 1) % ways) for d in range(ways)])  16.4 us
    all_to_all x1, starting transfers between devices, copy_for_each(): lax.all_to_all(jnp.broadcast_to(value[None], (count, *value.shape)), axis...  15.3 us
    ppermute x8, waiting for transfers between devices, collect(): lax.ppermute(going_up, axis, [(d, (d + 1) % ways) for d in range(ways)])  7.76 us
  transfers between devices with their start and end apart: 19, of which 8 were waited for; matrix products, arithmetic and copies ran while one was open for 6% of the time, Pallas kernels for 0%

profile of v1, /device:TPU:1, one launch (start us, length us, event | category | flops | bytes accessed | tf_op | source)
XLA Modules:
  0.0 292.1 jit_solution(8643809773301820393)
XLA Ops:
  7.2 0.9 copy.27
  9.1 1.2 reduce-window.6
  11.1 2.4 scatter_custom_fusion
  13.6 1.5 fusion.3
  15.1 1.5 fusion.5
  16.7 6.0 %gather_fusion = bf16[1024,2048]{1,0:T(8,128)(2,1)} fusion(bf16[257,2048]{1,0:T(8,128)(2,1)S(1)} %concatenate.67, s32[1024]{0:T(1024)S(1)} %fusion.51), kind=kCustom, calls=%fused_computation | custom fusion | bytes 8392704 | tf_op jit(solution)/shard_map/gather | solution.py:156
  22.8 1.1 constant_dynamic-slice_fusion
  23.9 38.9 %all_to_all.15 = bf16[32,32,128]{2,1,0:T(8,128)(2,1)} all-to-all(bf16[32,32,128]{2,1,0:T(8,128)(2,1)S(1)} %constant_dynamic-slice_fusion), channel_id=1, replica_groups=mesh['ep'=32,'tp'=16] {'ep'}, dimensions={0} | all-to-all | bytes 524288 | tf_op jit(solution)/shard_map/all_to_all | solution.py:161
  63.1 1.5 convolution_convert_fusion.2
  64.7 2.4 collective-permute-start
  70.2 54.8 %all-gather.2.cloned.1.call-done = bf16[32,32,2048]{2,1,0:T(8,128)(2,1)} async-done(((bf16[32,32,128]{2,1,0:T(8,128)(2,1)}), bf16[32,32,2048]{2,1,0:T(8,128)(2,1)}) %all-gather.2.cloned.1.call-update) | async-done | bytes 4194320 | tf_op jit(solution)/shard_map/all_gather | solution.py:162
  125.0 3.6 %fusion.20 = f32[1024,128]{1,0:T(8,128)S(1)} fusion(bf16[1024,2048]{1,0:T(8,128)(2,1)} %bitcast.63, bf16[1,2048,128]{2,1,0:T(8,128)(2,1)S(1)} %copy-done.4), kind=kOutput, calls=%fused_computation.33 | convolution fusion | flops 536870912 | bytes 5242880 | tf_op jit(solution)/shard_map/dot_general | solution.py:166
  129.2 1.4 constant_dynamic-update-slice_fusion.15
  130.5 2.0 copy-done.2
  132.5 2.8 collective-permute-start.1
  136.1 5.8 %collective-permute-start.2 = (bf16[1024,128]{1,0:T(8,128)(2,1)S(1)}, bf16[1024,128]{1,0:T(8,128)(2,1)S(1)}, u32[]{:S(2)}, u32[]{:S(2)}) collective-permute-start(bf16[1024,128]{1,0:T(8,128)(2,1)S(1)} %get-tuple-element.55), channel_id=1, source_target_pairs={{0,15},{1,0},{2,1},{3,2},{4,3},{5,4},{6,5},{7,6},{8,7},{9,8},{10,9... | collective-permute-start | bytes 786440 | tf_op jit(solution)/shard_map/ppermute | solution.py:19
  141.9 1.7 collective-permute-done.1
  143.5 1.9 collective-permute-start.3
  146.1 15.3 %all-to-all-start = ((f32[32,2,128]{2,1,0:T(2,128)}), f32[32,2,128]{2,1,0:T(2,128)S(1)}, u32[]{:S(2)}, u32[]{:S(2)}) async-start(f32[32,2,128]{2,1,0:T(2,128)} %broadcast_in_dim.50), calls=%async_computation | async-start | bytes 65536 | tf_op jit(solution)/shard_map/all_to_all | solution.py:34
  161.9 7.0 %collective-permute-start.4 = (bf16[1024,128]{1,0:T(8,128)(2,1)S(1)}, bf16[1024,128]{1,0:T(8,128)(2,1)S(1)}, u32[]{:S(2)}, u32[]{:S(2)}) collective-permute-start(bf16[1024,128]{1,0:T(8,128)(2,1)S(1)} %collective-permute-done.2), channel_id=1, source_target_pairs={{0,15},{1,0},{2,1},{3,2},{4,3},{5,4},{6,5},{7,6},{8,7},{9,8},{10,9... | collective-permute-start | bytes 786440 | tf_op jit(solution)/shard_map/ppermute | solution.py:19
  168.9 1.9 collective-permute-start.5
  170.8 2.6 all-to-all-done
  174.3 7.4 %collective-permute-start.6 = (bf16[1024,128]{1,0:T(8,128)(2,1)S(1)}, bf16[1024,128]{1,0:T(8,128)(2,1)S(1)}, u32[]{:S(2)}, u32[]{:S(2)}) collective-permute-start(bf16[1024,128]{1,0:T(8,128)(2,1)S(1)} %collective-permute-done.4), channel_id=1, source_target_pairs={{0,15},{1,0},{2,1},{3,2},{4,3},{5,4},{6,5},{7,6},{8,7},{9,8},{10,9... | collective-permute-start | bytes 786440 | tf_op jit(solution)/shard_map/ppermute | solution.py:19
  181.7 1.9 collective-permute-start.7
  183.7 0.8 constant_dynamic-update-slice_fusion.14
  184.5 1.7 collective-permute-done.6
  186.2 7.4 %collective-permute-start.8 = (bf16[1024,128]{1,0:T(8,128)(2,1)S(1)}, bf16[1024,128]{1,0:T(8,128)(2,1)S(1)}, u32[]{:S(2)}, u32[]{:S(2)}) collective-permute-start(bf16[1024,128]{1,0:T(8,128)(2,1)S(1)} %collective-permute-done.6), channel_id=1, source_target_pairs={{0,15},{1,0},{2,1},{3,2},{4,3},{5,4},{6,5},{7,6},{8,7},{9,8},{10,9... | collective-permute-start | bytes 786440 | tf_op jit(solution)/shard_map/ppermute | solution.py:19
  194.4 1.9 collective-permute-start.9
  196.3 0.8 constant_dynamic-update-slice_fusion.12
  197.1 0.8 constant_dynamic-update-slice_fusion.11
  197.9 6.9 %collective-permute-start.10 = (bf16[1024,128]{1,0:T(8,128)(2,1)S(1)}, bf16[1024,128]{1,0:T(8,128)(2,1)S(1)}, u32[]{:S(2)}, u32[]{:S(2)}) collective-permute-start(bf16[1024,128]{1,0:T(8,128)(2,1)S(1)} %collective-permute-done.8), channel_id=1, source_target_pairs={{0,15},{1,0},{2,1},{3,2},{4,3},{5,4},{6,5},{7,6},{8,7},{9,8},{10,9... | collective-permute-start | bytes 786440 | tf_op jit(solution)/shard_map/ppermute | solution.py:19
  204.8 0.8 constant_dynamic-update-slice_fusion.10
  205.6 1.9 collective-permute-start.11
  208.2 1.7 constant_dynamic-update-slice_fusion.8
  209.9 6.7 %collective-permute-start.12 = (bf16[1024,128]{1,0:T(8,128)(2,1)S(1)}, bf16[1024,128]{1,0:T(8,128)(2,1)S(1)}, u32[]{:S(2)}, u32[]{:S(2)}) collective-permute-start(bf16[1024,128]{1,0:T(8,128)(2,1)S(1)} %collective-permute-done.10), channel_id=1, source_target_pairs={{0,15},{1,0},{2,1},{3,2},{4,3},{5,4},{6,5},{7,6},{8,7},{9,8},{10,9... | collective-permute-start | bytes 786440 | tf_op jit(solution)/shard_map/ppermute | solution.py:19
  216.6 0.8 constant_dynamic-update-slice_fusion.7
  217.4 1.9 collective-permute-start.13
  220.8 6.7 %collective-permute-start.14 = (bf16[1024,128]{1,0:T(8,128)(2,1)S(1)}, bf16[1024,128]{1,0:T(8,128)(2,1)S(1)}, u32[]{:S(2)}, u32[]{:S(2)}) collective-permute-start(bf16[1024,128]{1,0:T(8,128)(2,1)S(1)} %collective-permute-done.12), channel_id=1, source_target_pairs={{0,15},{1,0},{2,1},{3,2},{4,3},{5,4},{6,5},{7,6},{8,7},{9,8},{10,9... | collective-permute-start | bytes 786440 | tf_op jit(solution)/shard_map/ppermute | solution.py:19
  227.5 0.8 constant_dynamic-update-slice_fusion.4
  228.3 2.1 collective-permute-start.15
  231.9 0.8 constant_dynamic-update-slice_fusion.1
  232.7 6.1 %collective-permute-done.15 = bf16[1024,128]{1,0:T(8,128)(2,1)S(1)} collective-permute-done((bf16[1024,128]{1,0:T(8,128)(2,1)S(1)}, bf16[1024,128]{1,0:T(8,128)(2,1)S(1)}, u32[]{:S(2)}, u32[]{:S(2)}) %collective-permute-start.15) | collective-permute-done | bytes 262176 | tf_op jit(solution)/shard_map/ppermute | solution.py:16
  239.5 4.2 %convolution_convert_fusion = bf16[1024,128]{1,0:T(8,128)(2,1)} fusion(bf16[1024,2048]{1,0:T(8,128)(2,1)} %constant_dynamic-update-slice_fusion, bf16[1,2048,128]{2,1,0:T(8,128)(2,1)S(1)} %copy-done.16), kind=kOutput, calls=%fused_computation.15 | convolution fusion | flops 537001984 | bytes 4980736 | tf_op jit(solution)/shard_map/dot_general | solution.py:170
  243.6 16.9 %all-to-all-start.2 = ((bf16[32,32,128]{2,1,0:T(8,128)(2,1)}), bf16[32,32,128]{2,1,0:T(8,128)(2,1)S(1)}, u32[]{:S(2)}, u32[]{:S(2)}) async-start(bf16[32,32,128]{2,1,0:T(8,128)(2,1)} %bitcast.17), calls=%async_computation.2 | async-start | bytes 524288 | tf_op jit(solution)/shard_map/all_to_all | solution.py:172
  260.8 2.2 fusion.37
  263.0 19.8 %all-to-all-done.2 = bf16[32,32,128]{2,1,0:T(8,128)(2,1)S(1)} async-done(((bf16[32,32,128]{2,1,0:T(8,128)(2,1)}), bf16[32,32,128]{2,1,0:T(8,128)(2,1)S(1)}, u32[]{:S(2)}, u32[]{:S(2)}) %all-to-all-start.2) | async-done | bytes 262176 | tf_op jit(solution)/shard_map/all_to_all | solution.py:172
  282.8 1.3 gather_fusion.1
  284.2 1.1 fusion.24
  (246 shorter events, 13.0 us)
Async XLA Ops:
  7.2 122.0 %copy-start = (bf16[1,2048,128]{2,1,0:T(8,128)(2,1)S(1)}, bf16[1,2048,128]{2,1,0:T(8,128)(2,1)}, u32[]{:S(2)}) copy-start(bf16[1,2048,128]{2,1,0:T(8,128)(2,1)} %param.30) | copy-start | bytes 1572868
  7.2 117.8 %all-gather.2.cloned.1.call-start = ((), (), s32[]{:S(2)}) async-start(), calls=%async_computation.3 | async-start | bytes 4456448 | tf_op jit(solution)/shard_map/all_gather | solution.py:162
  16.7 46.1 %copy-start.3 = (bf16[256,2048]{1,0:T(8,128)(2,1)S(1)}, bf16[256,2048]{1,0:T(8,128)(2,1)}, u32[]{:S(2)}) copy-start(bf16[256,2048]{1,0:T(8,128)(2,1)} %param.16) | copy-start | bytes 3145732
  16.7 46.4 %copy-start.20 = (f32[2048]{0:T(1024)S(1)}, f32[2048]{0:T(1024)}, u32[]{:S(2)}) copy-start(f32[2048]{0:T(1024)} %param.17) | copy-start | bytes 24580
  22.7 44.3 %copy-start.14 = (f32[256,2]{0,1:T(2,128)S(1)}, f32[256,2]{0,1:T(2,128)}, u32[]{:S(2)}) copy-start(f32[256,2]{0,1:T(2,128)} %param.28) | copy-start | bytes 6148
  22.7 44.3 %copy-start.15 = (f32[4,128]{1,0:T(4,128)S(1)}, f32[4,128]{1,0:T(4,128)}, u32[]{:S(2)}) copy-start(f32[4,128]{1,0:T(4,128)} %param.20) | copy-start | bytes 6148
  22.7 44.4 %copy-start.21 = (f32[128]{0:T(128)S(1)}, f32[128]{0:T(128)}, u32[]{:S(2)}) copy-start(f32[128]{0:T(128)} %param.23) | copy-start | bytes 1540
  22.7 45.2 %copy-start.17 = (f32[256,128]{1,0:T(8,128)S(1)}, f32[256,128]{1,0:T(8,128)}, u32[]{:S(2)}) copy-start(f32[256,128]{1,0:T(8,128)} %param.24) | copy-start | bytes 393220
  22.8 45.2 %copy-start.18 = (bf16[1,128,128]{2,1,0:T(8,128)(2,1)S(1)}, bf16[1,128,128]{2,1,0:T(8,128)(2,1)}, u32[]{:S(2)}) copy-start(bf16[1,128,128]{2,1,0:T(8,128)(2,1)} %param.21) | copy-start | bytes 98308
  22.8 45.4 %copy-start.19 = (bf16[1,128,128]{2,1,0:T(8,128)(2,1)S(1)}, bf16[1,128,128]{2,1,0:T(8,128)(2,1)}, u32[]{:S(2)}) copy-start(bf16[1,128,128]{2,1,0:T(8,128)(2,1)} %param.22) | copy-start | bytes 98308
  64.6 60.4 %copy-start.4 = (bf16[1,2048,128]{2,1,0:T(8,128)(2,1)S(1)}, bf16[1,2048,128]{2,1,0:T(8,128)(2,1)}, u32[]{:S(2)}) copy-start(bf16[1,2048,128]{2,1,0:T(8,128)(2,1)} %param.29) | copy-start | bytes 1572868
  64.7 3.2 %collective-permute-start = (bf16[3,128]{1,0:T(4,128)(2,1)S(1)}, bf16[3,128]{1,0:T(4,128)(2,1)S(1)}, u32[]{:S(2)}, u32[]{:S(2)}) collective-permute-start(bf16[3,128]{1,0:T(4,128)(2,1)S(1)} %slice.443), channel_id=1, source_target_pairs={{0,16},{16,32},{32,48},{48,64},{64,80},{80,96},{96,112},{112,128},... | collective-permute-start | bytes 2312 | tf_op jit(solution)/shard_map/ppermute | solution.py:29
  68.4 60.2 %copy-start.5 = (f32[256,128]{1,0:T(8,128)}, f32[256,128]{1,0:T(8,128)S(1)}, u32[]{:S(2)}) copy-start(f32[256,128]{1,0:T(8,128)S(1)} %fusion.16) | copy-start | bytes 393220
  70.0 59.1 %copy-start.6 = (f32[256,128]{1,0:T(8,128)}, f32[256,128]{1,0:T(8,128)S(1)}, u32[]{:S(2)}) copy-start(f32[256,128]{1,0:T(8,128)S(1)} %pad.130) | copy-start | bytes 393220
  70.2 59.0 %copy-start.8 = (f32[256,128]{1,0:T(8,128)}, f32[256,128]{1,0:T(8,128)S(1)}, u32[]{:S(2)}) copy-start(f32[256,128]{1,0:T(8,128)S(1)} %pad.129) | copy-start | bytes 393220
  125.0 4.1 %copy-start.1 = (bf16[32,32,2048]{2,1,0:T(8,128)(2,1)S(1)}, bf16[32,32,2048]{2,1,0:T(8,128)(2,1)}, u32[]{:S(2)}) copy-start(bf16[32,32,2048]{2,1,0:T(8,128)(2,1)} %all-gather.2.cloned.1.call-done) | copy-start | bytes 12582916
  129.2 6.1 %slice-start = ((f32[256,128]{1,0:T(8,128)}), f32[1,128]{1,0:T(1,128)S(1)}, s32[]{:S(2)}) async-start(f32[256,128]{1,0:T(8,128)} %copy-done.5), calls=%async_computation.4 | async-start | bytes 1024 | tf_op jit(solution)/shard_map/slice | solution.py:135
  130.5 2.0 copy-start.2
  132.5 11.0 %collective-permute-start.1 = (bf16[1024,128]{1,0:T(8,128)(2,1)S(1)}, bf16[1024,128]{1,0:T(8,128)(2,1)S(1)}, u32[]{:S(2)}, u32[]{:S(2)}) collective-permute-start(bf16[1024,128]{1,0:T(8,128)(2,1)S(1)} %get-tuple-element.55), channel_id=1, source_target_pairs={{0,1},{1,2},{2,3},{3,4},{4,5},{5,6},{6,7},{7,8},{8,9},{9,10},{10,1... | collective-permute-start | bytes 786440 | tf_op jit(solution)/shard_map/ppermute | solution.py:16
  135.4 0.7 copy-start.10
  136.0 5.8 %copy-start.12 = (f32[256,128]{1,0:T(8,128)}, f32[256,128]{1,0:T(8,128)S(1)}, u32[]{:S(2)}) copy-start(f32[256,128]{1,0:T(8,128)S(1)} %pad.113) | copy-start | bytes 393220
  136.1 25.8 %collective-permute-start.2 = (bf16[1024,128]{1,0:T(8,128)(2,1)S(1)}, bf16[1024,128]{1,0:T(8,128)(2,1)S(1)}, u32[]{:S(2)}, u32[]{:S(2)}) collective-permute-start(bf16[1024,128]{1,0:T(8,128)(2,1)S(1)} %get-tuple-element.55), channel_id=1, source_target_pairs={{0,15},{1,0},{2,1},{3,2},{4,3},{5,4},{6,5},{7,6},{8,7},{9,8},{10,9... | collective-permute-start | bytes 786440 | tf_op jit(solution)/shard_map/ppermute | solution.py:19
  143.5 25.3 %collective-permute-start.3 = (bf16[1024,128]{1,0:T(8,128)(2,1)S(1)}, bf16[1024,128]{1,0:T(8,128)(2,1)S(1)}, u32[]{:S(2)}, u32[]{:S(2)}) collective-permute-start(bf16[1024,128]{1,0:T(8,128)(2,1)S(1)} %collective-permute-done.1), channel_id=1, source_target_pairs={{0,1},{1,2},{2,3},{3,4},{4,5},{5,6},{6,7},{7,8},{8,9},{9,10},{10,1... | collective-permute-start | bytes 786440 | tf_op jit(solution)/shard_map/ppermute | solution.py:16
  146.1 27.4 %all-to-all-start = ((f32[32,2,128]{2,1,0:T(2,128)}), f32[32,2,128]{2,1,0:T(2,128)S(1)}, u32[]{:S(2)}, u32[]{:S(2)}) async-start(f32[32,2,128]{2,1,0:T(2,128)} %broadcast_in_dim.50), calls=%async_computation | async-start | bytes 65536 | tf_op jit(solution)/shard_map/all_to_all | solution.py:34
  161.9 12.4 %collective-permute-start.4 = (bf16[1024,128]{1,0:T(8,128)(2,1)S(1)}, bf16[1024,128]{1,0:T(8,128)(2,1)S(1)}, u32[]{:S(2)}, u32[]{:S(2)}) collective-permute-start(bf16[1024,128]{1,0:T(8,128)(2,1)S(1)} %collective-permute-done.2), channel_id=1, source_target_pairs={{0,15},{1,0},{2,1},{3,2},{4,3},{5,4},{6,5},{7,6},{8,7},{9,8},{10,9... | collective-permute-start | bytes 786440 | tf_op jit(solution)/shard_map/ppermute | solution.py:19
  168.9 12.8 %collective-permute-start.5 = (bf16[1024,128]{1,0:T(8,128)(2,1)S(1)}, bf16[1024,128]{1,0:T(8,128)(2,1)S(1)}, u32[]{:S(2)}, u32[]{:S(2)}) collective-permute-start(bf16[1024,128]{1,0:T(8,128)(2,1)S(1)} %collective-permute-done.3), channel_id=1, source_target_pairs={{0,1},{1,2},{2,3},{3,4},{4,5},{5,6},{6,7},{7,8},{8,9},{9,10},{10,1... | collective-permute-start | bytes 786440 | tf_op jit(solution)/shard_map/ppermute | solution.py:16
  174.3 12.0 %collective-permute-start.6 = (bf16[1024,128]{1,0:T(8,128)(2,1)S(1)}, bf16[1024,128]{1,0:T(8,128)(2,1)S(1)}, u32[]{:S(2)}, u32[]{:S(2)}) collective-permute-start(bf16[1024,128]{1,0:T(8,128)(2,1)S(1)} %collective-permute-done.4), channel_id=1, source_target_pairs={{0,15},{1,0},{2,1},{3,2},{4,3},{5,4},{6,5},{7,6},{8,7},{9,8},{10,9... | collective-permute-start | bytes 786440 | tf_op jit(solution)/shard_map/ppermute | solution.py:19
  181.7 12.7 %collective-permute-start.7 = (bf16[1024,128]{1,0:T(8,128)(2,1)S(1)}, bf16[1024,128]{1,0:T(8,128)(2,1)}, u32[]{:S(2)}, u32[]{:S(2)}) collective-permute-start(bf16[1024,128]{1,0:T(8,128)(2,1)S(1)} %collective-permute-done.5), channel_id=1, source_target_pairs={{0,1},{1,2},{2,3},{3,4},{4,5},{5,6},{6,7},{7,8},{8,9},{9,10},{10,1... | collective-permute-start | bytes 786440 | tf_op jit(solution)/shard_map/ppermute | solution.py:16
  183.7 55.8 %copy-start.16 = (bf16[1,2048,128]{2,1,0:T(8,128)(2,1)S(1)}, bf16[1,2048,128]{2,1,0:T(8,128)(2,1)}, u32[]{:S(2)}) copy-start(bf16[1,2048,128]{2,1,0:T(8,128)(2,1)} %param.31) | copy-start | bytes 1572868
  186.2 11.6 %collective-permute-start.8 = (bf16[1024,128]{1,0:T(8,128)(2,1)S(1)}, bf16[1024,128]{1,0:T(8,128)(2,1)S(1)}, u32[]{:S(2)}, u32[]{:S(2)}) collective-permute-start(bf16[1024,128]{1,0:T(8,128)(2,1)S(1)} %collective-permute-done.6), channel_id=1, source_target_pairs={{0,15},{1,0},{2,1},{3,2},{4,3},{5,4},{6,5},{7,6},{8,7},{9,8},{10,9... | collective-permute-start | bytes 786440 | tf_op jit(solution)/shard_map/ppermute | solution.py:19
  194.4 11.1 %collective-permute-start.9 = (bf16[1024,128]{1,0:T(8,128)(2,1)}, bf16[1024,128]{1,0:T(8,128)(2,1)S(1)}, u32[]{:S(2)}, u32[]{:S(2)}) collective-permute-start(bf16[1024,128]{1,0:T(8,128)(2,1)} %collective-permute-done.7), channel_id=1, source_target_pairs={{0,1},{1,2},{2,3},{3,4},{4,5},{5,6},{6,7},{7,8},{8,9},{9,10},{10,1... | collective-permute-start | bytes 786440 | tf_op jit(solution)/shard_map/ppermute | solution.py:16
  197.9 12.1 %collective-permute-start.10 = (bf16[1024,128]{1,0:T(8,128)(2,1)S(1)}, bf16[1024,128]{1,0:T(8,128)(2,1)S(1)}, u32[]{:S(2)}, u32[]{:S(2)}) collective-permute-start(bf16[1024,128]{1,0:T(8,128)(2,1)S(1)} %collective-permute-done.8), channel_id=1, source_target_pairs={{0,15},{1,0},{2,1},{3,2},{4,3},{5,4},{6,5},{7,6},{8,7},{9,8},{10,9... | collective-permute-start | bytes 786440 | tf_op jit(solution)/shard_map/ppermute | solution.py:19
  205.6 11.8 %collective-permute-start.11 = (bf16[1024,128]{1,0:T(8,128)(2,1)S(1)}, bf16[1024,128]{1,0:T(8,128)(2,1)S(1)}, u32[]{:S(2)}, u32[]{:S(2)}) collective-permute-start(bf16[1024,128]{1,0:T(8,128)(2,1)S(1)} %collective-permute-done.9), channel_id=1, source_target_pairs={{0,1},{1,2},{2,3},{3,4},{4,5},{5,6},{6,7},{7,8},{8,9},{9,10},{10,1... | collective-permute-start | bytes 786440 | tf_op jit(solution)/shard_map/ppermute | solution.py:16
  209.9 10.9 %collective-permute-start.12 = (bf16[1024,128]{1,0:T(8,128)(2,1)S(1)}, bf16[1024,128]{1,0:T(8,128)(2,1)S(1)}, u32[]{:S(2)}, u32[]{:S(2)}) collective-permute-start(bf16[1024,128]{1,0:T(8,128)(2,1)S(1)} %collective-permute-done.10), channel_id=1, source_target_pairs={{0,15},{1,0},{2,1},{3,2},{4,3},{5,4},{6,5},{7,6},{8,7},{9,8},{10,9... | collective-permute-start | bytes 786440 | tf_op jit(solution)/shard_map/ppermute | solution.py:19
  217.4 10.9 %collective-permute-start.13 = (bf16[1024,128]{1,0:T(8,128)(2,1)S(1)}, bf16[1024,128]{1,0:T(8,128)(2,1)S(1)}, u32[]{:S(2)}, u32[]{:S(2)}) collective-permute-start(bf16[1024,128]{1,0:T(8,128)(2,1)S(1)} %collective-permute-done.11), channel_id=1, source_target_pairs={{0,1},{1,2},{2,3},{3,4},{4,5},{5,6},{6,7},{7,8},{8,9},{9,10},{10,1... | collective-permute-start | bytes 786440 | tf_op jit(solution)/shard_map/ppermute | solution.py:16
  220.8 11.1 %collective-permute-start.14 = (bf16[1024,128]{1,0:T(8,128)(2,1)S(1)}, bf16[1024,128]{1,0:T(8,128)(2,1)S(1)}, u32[]{:S(2)}, u32[]{:S(2)}) collective-permute-start(bf16[1024,128]{1,0:T(8,128)(2,1)S(1)} %collective-permute-done.12), channel_id=1, source_target_pairs={{0,15},{1,0},{2,1},{3,2},{4,3},{5,4},{6,5},{7,6},{8,7},{9,8},{10,9... | collective-permute-start | bytes 786440 | tf_op jit(solution)/shard_map/ppermute | solution.py:19
  228.3 10.4 %collective-permute-start.15 = (bf16[1024,128]{1,0:T(8,128)(2,1)S(1)}, bf16[1024,128]{1,0:T(8,128)(2,1)S(1)}, u32[]{:S(2)}, u32[]{:S(2)}) collective-permute-start(bf16[1024,128]{1,0:T(8,128)(2,1)S(1)} %collective-permute-done.13), channel_id=1, source_target_pairs={{0,1},{1,2},{2,3},{3,4},{4,5},{5,6},{6,7},{7,8},{8,9},{9,10},{10,1... | collective-permute-start | bytes 786440 | tf_op jit(solution)/shard_map/ppermute | solution.py:16
  231.2 29.6 %copy-start.7 = (f32[256,128]{1,0:T(8,128)S(1)}, f32[256,128]{1,0:T(8,128)}, u32[]{:S(2)}) copy-start(f32[256,128]{1,0:T(8,128)} %copy-done.6) | copy-start | bytes 393220
  231.2 29.6 %copy-start.9 = (f32[256,128]{1,0:T(8,128)S(1)}, f32[256,128]{1,0:T(8,128)}, u32[]{:S(2)}) copy-start(f32[256,128]{1,0:T(8,128)} %copy-done.8) | copy-start | bytes 393220
  231.2 29.6 %copy-start.11 = (f32[256,128]{1,0:T(8,128)S(1)}, f32[256,128]{1,0:T(8,128)}, u32[]{:S(2)}) copy-start(f32[256,128]{1,0:T(8,128)} %copy-done.10) | copy-start | bytes 393220
  231.2 29.7 %copy-start.13 = (f32[256,128]{1,0:T(8,128)S(1)}, f32[256,128]{1,0:T(8,128)}, u32[]{:S(2)}) copy-start(f32[256,128]{1,0:T(8,128)} %copy-done.12) | copy-start | bytes 393220
  243.6 39.2 %all-to-all-start.2 = ((bf16[32,32,128]{2,1,0:T(8,128)(2,1)}), bf16[32,32,128]{2,1,0:T(8,128)(2,1)S(1)}, u32[]{:S(2)}, u32[]{:S(2)}) async-start(bf16[32,32,128]{2,1,0:T(8,128)(2,1)} %bitcast.17), calls=%async_computation.2 | async-start | bytes 524288 | tf_op jit(solution)/shard_map/all_to_all | solution.py:172
Sparse Core Ops, SparseCore 0:
  62.9 62.0 all-gather.1
